TPU v7x, 32 devices: a whole 2x2x4 slice. The times are simulated.
32 devices in a mesh: ep: 16 (over z, y, x), tp: 2 (over core).
Axes of the slice: x: 2, y: 2, z: 4, core: 2. Of those that a mesh axis runs over, the one named last changes fastest.
Arguments:
- tokens: bfloat16 [4096, 2048], P('ep', 'tp'), may hold values from -6 to 6
- experts: int32 [4096, 16], P('ep'), may hold values from 0 to 65535, as said below
- weights: float32 [4096, 16], P('ep'), may hold values from 0.05 to 1
- up_table: bfloat16 [65536, 2048], P('ep', 'tp'), may hold values from -0.125 to 0.125
- out_table: bfloat16 [65536, 2048], P('ep', 'tp')
- gain: float32 [2048], P('tp'), may hold values from 0.1 to 1.9
Outputs:
- normed: bfloat16 [4096, 2048], P('ep', 'tp')
Inputs may be any that keep to these rules, and one draw needn't show every extreme that they name: An expert number e lies with index e // 4096 of ep. Among the rows of one index of ep, at most 512 chosen experts lie with any one index of ep, and in every draw some index of ep receives exactly 512 from every index.
All inputs are finite; a program needn't handle non-finite values.
Results may differ from a plain program's by a relative error of at most 0.006.
Values may be sent and summed in bfloat16 or wider, within the bound.
A program may use at most 128 MiB of HBM per device.

v0:
```python
import functools
import math

import jax
import jax.numpy as jnp
from jax import lax
from jax.experimental import pallas as pl
from jax.experimental.pallas import tpu as pltpu
from jax.sharding import PartitionSpec as P

LANES = 128


def owner_ranks(owner, n_ep):
    request_list = owner.shape[0]
    block_len = 512
    block_count = request_list // block_len
    onehot = (owner[:, None] == jnp.arange(n_ep, dtype=jnp.int32)[None, :]).astype(jnp.bfloat16)
    onehot_blocks = onehot.reshape(block_count, block_len, n_ep)
    row_pos = jnp.arange(block_len, dtype=jnp.int32)
    lower = (row_pos[:, None] >= row_pos[None, :]).astype(jnp.bfloat16)
    within = jnp.einsum("ij,bjn->bin", lower, onehot_blocks, preferred_element_type=jnp.float32)
    totals = within[:, block_len - 1, :]
    before = jnp.cumsum(totals, axis=0) - totals
    counted = jnp.sum((within + before[:, None, :]) * onehot_blocks.astype(jnp.float32), axis=2)
    return counted.reshape(request_list).astype(jnp.int32) - 1


def dots_kernel(capacity, place_ref, row_ref, tok_ref, up_ref, dot_ref, prod):
    sub = tok_ref.shape[1]
    base = pl.program_id(0) * capacity
    unroll = 32
    for block in range(capacity // LANES):

        def some(g, carry):
            for u in range(unroll):
                k = g * unroll + u
                at = base + block * LANES + k
                a = tok_ref[place_ref[at]].astype(jnp.float32)
                b = up_ref[row_ref[at]].astype(jnp.float32)
                prod[pl.ds(pl.multiple_of(k * sub, sub), sub), :] = a * b
            return carry

        lax.fori_loop(0, LANES // unroll, some, 0)
        if sub == 1:
            total = prod[...]
        else:
            total = prod[pl.ds(0, LANES, stride=sub), :]
            for s in range(1, sub):
                total = total + prod[pl.ds(s, LANES, stride=sub), :]
        dot_ref[0, pl.ds(block, 1), :] = jnp.sum(total.T, axis=0, keepdims=True)


def request_dots(places, rows, tok_all, up, capacity, n_ep):
    rows_held, sub, _ = up.shape
    tok_rows = tok_all.shape[0] // n_ep
    return pl.pallas_call(
        functools.partial(dots_kernel, capacity),
        grid_spec=pltpu.PrefetchScalarGridSpec(
            num_scalar_prefetch=2,
            grid=(n_ep,),
            in_specs=[
                pl.BlockSpec((tok_rows, sub, LANES), lambda i, p, r: (i, 0, 0)),
                pl.BlockSpec((rows_held, sub, LANES), lambda i, p, r: (0, 0, 0)),
            ],
            out_specs=pl.BlockSpec((1, capacity // LANES, LANES), lambda i, p, r: (i, 0, 0)),
            scratch_shapes=[pltpu.VMEM((LANES * sub, LANES), jnp.float32)],
        ),
        out_shape=jax.ShapeDtypeStruct((n_ep, capacity // LANES, LANES), jnp.float32),
        name="request_dots",
    )(places, rows, tok_all, up)


def mix_kernel(capacity, group, place_ref, row_ref, coef_ref, table_ref, mix_ref, acc):
    first = pl.program_id(0) * group

    def clear(i, carry):
        acc[pl.ds(i * LANES, LANES)] = jnp.zeros((LANES,) + acc.shape[1:], acc.dtype)
        return carry

    lax.fori_loop(0, acc.shape[0] // LANES, clear, 0)

    def step(j, carry):
        places, sums = [], []
        for s in range(group):
            at = (first + s) * capacity + j
            place = place_ref[at]
            row = table_ref[row_ref[at]].astype(jnp.float32)
            places.append(place)
            sums.append(acc[place] + coef_ref[at] * row)
        for place, total in zip(places, sums):
            acc[place] = total
        return carry

    lax.fori_loop(0, capacity, step, 0)

    def emit(i, carry):
        mix_ref[pl.ds(i * LANES, LANES)] = acc[pl.ds(i * LANES, LANES)].astype(mix_ref.dtype)
        return carry

    lax.fori_loop(0, acc.shape[0] // LANES, emit, 0)


def mix_rows(places, rows, coef, table, capacity, n_ep, tok_rows, group):
    rows_held, sub, _ = table.shape
    return pl.pallas_call(
        functools.partial(mix_kernel, capacity, group),
        grid_spec=pltpu.PrefetchScalarGridSpec(
            num_scalar_prefetch=3,
            grid=(n_ep // group,),
            in_specs=[pl.BlockSpec((rows_held, sub, LANES), lambda i, p, r, c: (0, 0, 0))],
            out_specs=pl.BlockSpec((group * tok_rows, sub, LANES), lambda i, p, r, c: (i, 0, 0)),
            scratch_shapes=[pltpu.VMEM((group * tok_rows, sub, LANES), jnp.float32)],
        ),
        out_shape=jax.ShapeDtypeStruct((n_ep * tok_rows, sub, LANES), jnp.bfloat16),
        name="mix_rows",
    )(places, rows, coef, table)


def body(tokens, experts, weights, up_table, out_table, gain):
    n_ep = lax.axis_size("ep")
    tok_rows, width = tokens.shape
    slots = experts.shape[1]
    rows_held = up_table.shape[0]
    sub = width // LANES
    request_list = tok_rows * slots
    capacity = 2 * request_list // n_ep
    tok_all = lax.all_gather(tokens.reshape(tok_rows, sub, LANES), "ep", axis=0, tiled=True)
    flat = experts.reshape(-1)
    owner = flat // rows_held
    local_row = flat - owner * rows_held
    position = owner * capacity + owner_ranks(owner, n_ep)
    token_of = jnp.arange(request_list, dtype=jnp.int32) // slots
    send_words = (
        jnp.zeros((n_ep * capacity,), jnp.int32)
        .at[position]
        .set(token_of * rows_held + local_row, unique_indices=True)
    )
    send_weights = (
        jnp.zeros((n_ep * capacity,), jnp.float32)
        .at[position]
        .set(weights.reshape(-1), unique_indices=True)
    )
    words = lax.all_to_all(send_words.reshape(n_ep, capacity), "ep", 0, 0, tiled=True)
    token_at = words // rows_held
    row_at = (words % rows_held).reshape(-1)
    group = math.gcd(n_ep, 16)
    first = (jnp.arange(n_ep, dtype=jnp.int32) % group) * tok_rows
    place_at = (token_at + first[:, None]).reshape(-1)
    scales = lax.all_to_all(send_weights.reshape(n_ep, capacity), "ep", 0, 0, tiled=True)
    up = up_table.reshape(rows_held, sub, LANES)
    out = out_table.reshape(rows_held, sub, LANES)
    partial_value = request_dots(token_at.reshape(-1), row_at, tok_all, up, capacity, n_ep)
    dot = lax.psum(partial_value, "tp")
    coef = (scales.reshape(dot.shape) * jax.nn.gelu(dot)).reshape(-1)
    part = mix_rows(place_at, row_at, coef, out, capacity, n_ep, tok_rows, group)
    mixed = lax.psum_scatter(part, "ep", scatter_dimension=0, tiled=True).astype(jnp.float32)
    square = lax.psum(jnp.sum(mixed * mixed, axis=(1, 2)), "tp")
    scale = lax.rsqrt(square / (width * lax.axis_size("tp")) + 1e-06)
    normed = mixed * scale[:, None, None] * gain.reshape(1, sub, LANES)
    return normed.astype(jnp.bfloat16).reshape(tok_rows, width)


def solution(mesh):
    placed = (P("ep", "tp"), P("ep", None), P("ep", None), P("ep", "tp"), P("ep", "tp"), P("tp"))
    return jax.shard_map(body, mesh=mesh, in_specs=placed, out_specs=P("ep", "tp"), check_vma=False)
```

profile of v0, /device:TPU:9, one launch (start us, length us, event | category | flops | bytes accessed | tf_op | source)
XLA Modules:
  0.0 395.2 jit_solution(16698907273081976393)
XLA Ops:
  6.5 0.0 all-gather.2.cloned.1.call-start
  6.5 1.9 copy.17
  8.5 0.0 all-gather.2.cloned.1.call-update
  8.5 0.8 copy.11
  9.3 0.1 reshape.190
  9.4 0.1 reshape.189
  9.5 0.1 reshape.188
  9.7 0.3 convolution_bitcast_fusion
  10.0 0.2 fusion.35
  10.2 0.1 multiply_reduce_fusion
  10.4 0.1 compare_select_fusion
  10.5 16.1 %scatter_custom_fusion = s32[8192]{0:T(1024)} fusion(s32[4096]{0:T(1024)S(1)} %bitcast.44, s32[4096]{0:T(1024)S(1)} %fusion.20, s32[]{:T(128)} %constant.74.clone.1), kind=kCustom, calls=%fused_computation.65 | custom fusion | bytes 32772 | tf_op jit(solution)/shard_map/scatter | solution.py:137
  26.5 6.7 %all-to-all-start = ((s32[16,1,512]{2,1,0:T(1,128)}), s32[16,1,512]{2,1,0:T(1,128)S(1)}, u32[]{:S(2)}, u32[]{:S(2)}) async-start(s32[16,1,512]{2,1,0:T(1,128)} %bitcast.3), calls=%async_computation | async-start | bytes 65536 | tf_op jit(solution)/shard_map/all_to_all | solution.py:144
  33.2 0.1 broadcast_bitcast_fusion
  33.3 0.8 copy.14
  34.1 0.1 reshape.210
  34.2 8.8 %copy.18 = bf16[512,8,8,128]{3,2,1,0:T(8,128)(2,1)} copy(bf16[512,8,8,128]{3,1,2,0:T(8,128)(2,1)} %bitcast.34) | data formatting | bytes 16777216
  43.0 8.8 %copy.19 = bf16[512,8,8,128]{3,2,1,0:T(8,128)(2,1)} copy(bf16[512,8,8,128]{3,1,2,0:T(8,128)(2,1)} %bitcast.35) | data formatting | bytes 16777216
  51.8 16.1 %scatter_custom_fusion.1 = f32[8192]{0:T(1024)} fusion(s32[4096]{0:T(1024)S(1)} %bitcast.45, f32[4096]{0:T(1024)S(1)} %reshape.210, f32[]{:T(128)} %constant.80.clone.1), kind=kCustom, calls=%fused_computation.59 | custom fusion | bytes 32772 | tf_op jit(solution)/shard_map/scatter | solution.py:142
  67.9 0.0 all-to-all-done
  67.9 6.4 %all-to-all-start.1 = ((f32[16,1,512]{2,1,0:T(1,128)}), f32[16,1,512]{2,1,0:T(1,128)S(1)}, u32[]{:S(2)}, u32[]{:S(2)}) async-start(f32[16,1,512]{2,1,0:T(1,128)} %bitcast.5), calls=%async_computation.1 | async-start | bytes 65536 | tf_op jit(solution)/shard_map/all_to_all | solution.py:150
  74.3 0.0 reduce-scatter.2.cloned.1.call-start
  74.3 0.7 add_select_fusion.1
  75.0 46.1 %all-gather.2.cloned.1.call-done.tok_ref = bf16[4096,8,128]{2,1,0:T(8,128)(2,1)} async-done(((bf16[256,8,128]{2,1,0:T(8,128)(2,1)}), bf16[4096,8,128]{2,1,0:T(8,128)(2,1)}) %all-gather.2.cloned.1.call-update) | async-done | bytes 8388624 | tf_op jit(solution)/shard_map/all_gather | solution.py:128
  121.1 35.3 %request_dots.1 = f32[16,4,128]{2,1,0:T(4,128)} custom-call(s32[8192]{0:T(1024)} %get-tuple-element.5.place_ref, s32[8192]{0:T(1024)} %get-tuple-element.7.row_ref, bf16[4096,8,128]{2,1,0:T(8,128)(2,1)} %all-gather.2.cloned.1.call-done.tok_ref, bf16[4096,8,128]{2,1,0:T(8,128)(2,1)} %bitcast.33), custom_call_target="tpu_custom_call" | custom-call | tf_op jit(solution)/shard_map/request_dots/pallas_call | solution.py:57
  156.4 6.5 %psum.14 = f32[16,4,128]{2,1,0:T(4,128)S(1)} all-reduce(f32[16,4,128]{2,1,0:T(4,128)} %request_dots.1), channel_id=1, replica_groups=mesh['ep'=16,'tp'=2] {'tp'}, use_global_device_ids=true, to_apply=%region_4.5 | all-reduce | flops 8192 | bytes 65536 | tf_op jit(solution)/shard_map/psum | solution.py:154
  162.9 0.0 all-to-all-done.1
  162.9 0.6 fusion.15
  163.5 41.3 %mix_rows.1 = bf16[4096,8,128]{2,1,0:T(8,128)(2,1)} custom-call(s32[8192]{0:T(1024)} %get-tuple-element.6.place_ref, s32[8192]{0:T(1024)} %get-tuple-element.7.row_ref, f32[8192]{0:T(1024)} %bitcast.39, bf16[4096,8,128]{2,1,0:T(8,128)(2,1)} %bitcast.32), custom_call_target="tpu_custom_call" | custom-call | tf_op jit(solution)/shard_map/mix_rows/pallas_call | solution.py:106
  204.9 0.0 copy-start
  204.9 0.0 reduce-scatter.2.cloned.1.call-update
  204.9 176.3 %reduce-scatter.2.cloned.1.call-done = bf16[256,8,128]{2,1,0:T(8,128)(2,1)} async-done(((bf16[4096,8,128]{2,1,0:T(8,128)(2,1)}), bf16[256,8,128]{2,1,0:T(8,128)(2,1)}) %reduce-scatter.2.cloned.1.call-update) | async-done | bytes 524304 | tf_op jit(solution)/shard_map/reduce_scatter | solution.py:157
  381.2 2.1 fusion
  383.3 2.9 psum.15
  386.1 0.0 copy-done
  386.1 1.4 fusion.2
  387.5 0.9 copy.22
  (7 shorter events, 0.1 us)
Async XLA Ops:
  6.5 114.6 %all-gather.2.cloned.1.call-start = ((), (), s32[]{:S(2)}) async-start(), calls=%async_computation.3 | async-start | bytes 8912896 | tf_op jit(solution)/shard_map/all_gather | solution.py:128
  26.5 41.4 %all-to-all-start = ((s32[16,1,512]{2,1,0:T(1,128)}), s32[16,1,512]{2,1,0:T(1,128)S(1)}, u32[]{:S(2)}, u32[]{:S(2)}) async-start(s32[16,1,512]{2,1,0:T(1,128)} %bitcast.3), calls=%async_computation | async-start | bytes 65536 | tf_op jit(solution)/shard_map/all_to_all | solution.py:144
  67.9 95.0 %all-to-all-start.1 = ((f32[16,1,512]{2,1,0:T(1,128)}), f32[16,1,512]{2,1,0:T(1,128)S(1)}, u32[]{:S(2)}, u32[]{:S(2)}) async-start(f32[16,1,512]{2,1,0:T(1,128)} %bitcast.5), calls=%async_computation.1 | async-start | bytes 65536 | tf_op jit(solution)/shard_map/all_to_all | solution.py:150
  74.3 306.9 %reduce-scatter.2.cloned.1.call-start = ((), (), s32[]{:S(2)}) async-start(), calls=%async_computation.4 | async-start | bytes 8912896 | tf_op jit(solution)/shard_map/reduce_scatter | solution.py:157
  204.9 181.2 %copy-start = (f32[1024]{0:T(1024)S(1)}, f32[1024]{0:T(1024)}, u32[]{:S(2)}) copy-start(f32[1024]{0:T(1024)} %param.11) | copy-start | bytes 12292
Sparse Core Ops, SparseCore 0:
  10.1 110.9 all-gather.1
  205.0 176.1 reduce-scatter.1
where the time goes:
time: 400 us; the launch traced here: 395 us
  waiting for transfers between devices  222 us (56%)
  Pallas kernels  76.6 us (19%)
  local copies, waits for them, and re-layouts  54.7 us (14%)
  between operations  13.5 us (3%)
  starting transfers between devices  13.1 us (3%)
  blocking collectives  9.31 us (2%)
  other arithmetic  5.23 us (1%)
    reduce_scatter x1, waiting for transfers between devices, body(): lax.psum_scatter(part, 'ep', scatter_dimension=0, tiled=True)  176 us
    all_gather x1, waiting for transfers between devices, body(): lax.all_gather(tokens.reshape(tok_rows, sub, LANES), 'ep', axis=0, tiled=...  46.1 us
    pallas_call x1, Pallas kernels, mix_rows(): pl.pallas_call(functools.partial(mix_kernel, capacity, group), grid_spec=...  41.3 us
    pallas_call x1, Pallas kernels, request_dots(): pl.pallas_call(functools.partial(dots_kernel, capacity), grid_spec=pltpu....  35.3 us
    unnamed x11, local copies, waits for them, and re-layouts  22.2 us
    scatter x1, local copies, waits for them, and re-layouts, body(): send_words = jnp.zeros((n_ep * capacity,), jnp.int32).at[position].set(to...  16.1 us
    scatter x1, local copies, waits for them, and re-layouts, body(): send_weights = jnp.zeros((n_ep * capacity,), jnp.float32).at[position].se...  16.1 us
  transfers between devices with their start and end apart: 4, of which 2 were waited for; matrix products, arithmetic and copies ran while one was open for 13% of the time, Pallas kernels for 9%

commit v1 on v0

v1 whole, which is shorter than its diff:
```python
import functools
import itertools

import jax
import jax.numpy as jnp
import numpy as np
from jax import lax
from jax.experimental import pallas as pl
from jax.experimental.pallas import tpu as pltpu
from jax.sharding import PartitionSpec as P

LANES = 128
MESH = pl.DeviceIdType.MESH
NT = (((1,), (1,)), ((), ()))
VMEM_LIMIT = 60 * 1024 * 1024


def ep_dims(mesh):
    n = mesh.shape["ep"]
    devices = np.moveaxis(mesh.devices, mesh.axis_names.index("ep"), 0).reshape(n, -1)[:, 0]
    coords = [getattr(d, "coords", None) for d in devices]
    if any(c is None for c in coords):
        return (n,)
    axes = []
    for a in range(len(coords[0])):
        values = [c[a] for c in coords]
        size = len(set(values))
        if size > 1:
            stride = next(i for i in range(n) if values[i] != values[0])
            axes.append((stride, size, [v - min(values) for v in values]))
    axes.sort(key=lambda t: -t[0])
    dims = tuple(size for _, size, _ in axes)
    if int(np.prod(dims)) != n:
        return (n,)
    for i in range(n):
        if any((i // stride) % size != values[i] for stride, size, values in axes):
            return (n,)
    return dims


def tree_plans(dims, rows):
    k = len(dims)
    if k == 3 and rows % 128 == 0:
        long, mid, last = sorted(range(3), key=lambda i: -dims[i])
        unit = rows // 8
        plans = [
            ((long, mid, last), 3 * unit),
            ((long, last, mid), 3 * unit),
            ((last, mid, long), unit),
            ((mid, last, long), unit),
        ]
    elif k == 2 and rows % 32 == 0:
        plans = [((0, 1), rows // 2), ((1, 0), rows // 2)]
    else:
        plans = [(tuple(range(k)), rows)]
    out, first = [], 0
    for order, count in plans:
        out.append((order, first, count))
        first += count
    return out


class Place:
    def __init__(self, dims):
        self.dims = dims
        self.strides = [int(np.prod(dims[i + 1 :])) for i in range(len(dims))]
        self.e = lax.axis_index("ep")
        self.tp = lax.axis_index("tp")
        self.at = [(self.e // st) % n for st, n in zip(self.strides, dims)]

    def near(self, dim, k):
        m, n = self.at[dim], self.dims[dim]
        if k == 0:
            return m
        if n == 2:
            return 1 - m
        below, above = m, n - 1 - m
        low = jnp.minimum(below, above)
        hop = (k + 1) // 2
        alternate = m + hop if k % 2 else m - hop
        far = jnp.where(below < above, m + (k - low), m - (k - low))
        return jnp.where(k <= 2 * low, alternate, far)

    def flat(self, coords):
        total = 0
        for c, st in zip(coords, self.strides):
            total = total + c * st
        return total

    def moved(self, dim, to):
        return self.e + (to - self.at[dim]) * self.strides[dim]


def tree_events(order, dims):
    events = []
    for j in range(len(order)):
        heads = [range(dims[order[i]]) for i in range(j)] + [range(1, dims[order[j]])]
        for ks in itertools.product(*heads):
            events.append((j, ks))
    return events


def event_block(place, order, j, ks):
    coords = list(place.at)
    for i in range(j + 1):
        coords[order[i]] = place.near(order[i], ks[i])
    return coords


def tree_neighbors(place, order, j, coords):
    out = []
    for l in range(max(j, 0), len(order)):
        dim = order[l]
        n, m = place.dims[dim], place.at[dim]
        if l == j:
            if n > 2:
                to = m + jnp.where(m > coords[dim], 1, -1)
                out.append((l, to, (to >= 0) & (to < n)))
        elif n == 2:
            out.append((l, 1 - m, None))
        else:
            out.append((l, m + 1, m + 1 < n))
            out.append((l, m - 1, m > 0))
    return out


def schedule(plans, dims):
    keyed = []
    for v, (order, _, count) in enumerate(plans):
        seen = {}
        for j, ks in tree_events(order, dims):
            dist = sum((k + 1) // 2 if dims[order[i]] > 2 else k for i, k in enumerate(ks))
            before = seen.get(j, 0)
            seen[j] = before + 1
            keyed.append(((dist + before) * 1.0 + 0.01 * j, v, j, ks))
    keyed.sort(key=lambda t: t[0])
    return [(v, j, ks) for _, v, j, ks in keyed]


def maybe(pred, fn):
    if pred is None:
        fn()
    else:
        pl.when(pred)(fn)


def route_kernel(n_ep, cap, rows_held, experts_ref, weights_ref, list_ref):
    slots, tok_rows = experts_ref.shape
    col = lax.broadcasted_iota(jnp.int32, (tok_rows, tok_rows), 1)
    row = lax.broadcasted_iota(jnp.int32, (tok_rows, tok_rows), 0)
    before = (row < col).astype(jnp.float32).astype(jnp.bfloat16)
    owners = lax.broadcasted_iota(jnp.int32, (n_ep, tok_rows), 0)
    places = lax.broadcasted_iota(jnp.int32, (cap, tok_rows), 0)
    token = lax.broadcasted_iota(jnp.int32, (1, tok_rows), 1)
    base = jnp.zeros((n_ep, 1), jnp.float32)
    total = jnp.zeros((6 * n_ep, cap), jnp.float32)
    for k in range(slots):
        e = experts_ref[k : k + 1, :]
        owner = e // rows_held
        mine = owner == owners
        ones = jnp.where(mine, 1.0, 0.0)
        ahead = jnp.dot(ones.astype(jnp.bfloat16), before, preferred_element_type=jnp.float32) + base
        base = base + jnp.sum(ones, axis=1, keepdims=True)
        rank = jnp.sum(jnp.where(mine, ahead, 0.0), axis=0, keepdims=True).astype(jnp.int32)
        at = jnp.where(rank == places, 1.0, 0.0).astype(jnp.bfloat16)
        word = token * rows_held + (e - owner * rows_held)
        w = weights_ref[k : k + 1, :]
        w0 = w.astype(jnp.bfloat16).astype(jnp.float32)
        w1 = (w - w0).astype(jnp.bfloat16).astype(jnp.float32)
        w2 = w - w0 - w1
        parts = [(word & 255), ((word >> 8) & 255), (word >> 16)]
        parts = [p.astype(jnp.float32) for p in parts] + [w0, w1, w2]
        lhs = jnp.concatenate([jnp.where(mine, p, 0.0) for p in parts], axis=0).astype(jnp.bfloat16)
        total = total + lax.dot_general(lhs, at, NT, preferred_element_type=jnp.float32)
    take = lambda i: total[i * n_ep : (i + 1) * n_ep, :]
    list_ref[:, 0, :] = take(0) + 256.0 * take(1) + 65536.0 * take(2)
    list_ref[:, 1, :] = take(3) + take(4) + take(5)


def route(experts_t, weights_t, n_ep, cap, rows_held):
    return pl.pallas_call(
        functools.partial(route_kernel, n_ep, cap, rows_held),
        out_shape=jax.ShapeDtypeStruct((n_ep, 2, cap), jnp.float32),
        compiler_params=pltpu.CompilerParams(vmem_limit_bytes=VMEM_LIMIT),
        name="route",
    )(experts_t, weights_t)


def count_sends(plans, dims):
    total = 0
    for order, _, _ in plans:
        for j, _ in [(-1, ())] + tree_events(order, dims):
            for l in range(max(j, 0), len(order)):
                big = dims[order[l]] > 2
                total += (1 if big else 0) if l == j else (2 if big else 1)
    return total


def gather_kernel(dims, plans, tok_ref, list_ref, all_ref, lists_ref, ssem, rsem, lssem, lrsem):
    place = Place(dims)
    n_ep = all_ref.shape[0]
    me = place.e
    barrier = pltpu.get_barrier_semaphore()
    for o in range(1, n_ep):
        pl.semaphore_signal(barrier, inc=1, device_id=((me + o) % n_ep, place.tp), device_id_type=MESH)
    pl.semaphore_wait(barrier, n_ep - 1)

    list_copies = []
    for o in range(1, n_ep):
        to = (me + o) % n_ep
        copy = pltpu.make_async_remote_copy(
            src_ref=list_ref.at[to],
            dst_ref=lists_ref.at[me],
            send_sem=lssem.at[o],
            recv_sem=lrsem.at[o],
            device_id=(to, place.tp),
            device_id_type=MESH,
        )
        copy.start()
        list_copies.append(copy)

    sends = []

    def forward(v, j, coords, src):
        order, first, count = plans[v]
        s = place.flat(coords)
        for l, to, pred in tree_neighbors(place, order, j, coords):
            copy = pltpu.make_async_remote_copy(
                src_ref=src,
                dst_ref=all_ref.at[s, pl.ds(first, count)],
                send_sem=ssem.at[len(sends)],
                recv_sem=rsem.at[v, s],
                device_id=(place.moved(order[l], to), place.tp),
                device_id_type=MESH,
            )
            maybe(pred, copy.start)
            sends.append((pred, copy))

    for v, (order, first, count) in enumerate(plans):
        forward(v, -1, place.at, tok_ref.at[pl.ds(first, count)])
    all_ref[me] = tok_ref[...]
    lists_ref[me] = list_ref[me]
    for v, j, ks in schedule(plans, dims):
        order, first, count = plans[v]
        coords = event_block(place, order, j, ks)
        s = place.flat(coords)
        block = all_ref.at[s, pl.ds(first, count)]
        pltpu.make_async_remote_copy(
            src_ref=block,
            dst_ref=block,
            send_sem=ssem.at[0],
            recv_sem=rsem.at[v, s],
            device_id=(me, place.tp),
            device_id_type=MESH,
        ).wait_recv()
        forward(v, j, coords, block)
    for copy in list_copies:
        copy.wait()
    for pred, copy in sends:
        maybe(pred, copy.wait_send)


def gather_tokens(tokens, lists, dims, plans):
    n_ep = int(np.prod(dims))
    vmem = pl.BlockSpec(memory_space=pltpu.VMEM)
    return pl.pallas_call(
        functools.partial(gather_kernel, dims, plans),
        out_shape=(
            jax.ShapeDtypeStruct((n_ep,) + tokens.shape, tokens.dtype),
            jax.ShapeDtypeStruct(lists.shape, lists.dtype),
        ),
        in_specs=[vmem, vmem],
        out_specs=(vmem, vmem),
        scratch_shapes=[
            pltpu.SemaphoreType.DMA((count_sends(plans, dims),)),
            pltpu.SemaphoreType.DMA((len(plans), n_ep)),
            pltpu.SemaphoreType.DMA((n_ep,)),
            pltpu.SemaphoreType.DMA((n_ep,)),
        ],
        compiler_params=pltpu.CompilerParams(
            collective_id=0, has_side_effects=True, vmem_limit_bytes=VMEM_LIMIT
        ),
        name="gather_tokens",
    )(tokens, lists)


def load_table(table_ref, flat, stage, sem):
    rows, width = table_ref.shape
    sub = width // LANES
    step = stage.shape[1]
    chunks = rows // step

    def copy(i, slot):
        return pltpu.make_async_copy(table_ref.at[pl.ds(i * step, step)], stage.at[slot], sem.at[slot])

    copy(0, 0).start()
    for i in range(chunks):
        slot = i % 2
        if i + 1 < chunks:
            copy(i + 1, 1 - slot).start()
        copy(i, slot).wait()

        def spread(g, carry):
            r = pl.multiple_of(g * 16, 16)
            for c in range(sub):
                x = stage[slot, pl.ds(r, 16), c * LANES : (c + 1) * LANES].astype(jnp.float32)
                for h in range(2):
                    first = (i * step + r + 8 * h) * sub + c
                    flat[pl.ds(first, 8, stride=sub), :] = x[8 * h : 8 * h + 8, :]
            return carry

        lax.fori_loop(0, step // 16, spread, 0)


def take_rows(row_ref, first, cap, sub, flat, picked, packed):
    unroll = 32

    def some(g, carry):
        for u in range(unroll):
            r = g * unroll + u
            at = pl.multiple_of(row_ref[first + r], sub)
            picked[pl.ds(pl.multiple_of(r * sub, sub), sub), :] = flat[pl.ds(at, sub), :]
        return carry

    lax.fori_loop(0, cap // unroll, some, 0)
    for c in range(sub):
        lines = picked[pl.ds(c, cap, stride=sub), :] if sub > 1 else picked[...]
        packed[:, c * LANES : (c + 1) * LANES] = lines.astype(jnp.bfloat16)


def hits(list_ref, s, tok_rows, rows_held):
    cap = list_ref.shape[2]
    word = list_ref[s, 0:1, :].astype(jnp.int32)
    return (word // rows_held) == lax.broadcasted_iota(jnp.int32, (tok_rows, cap), 0)


def dots_kernel(row_ref, list_ref, tok_ref, table_ref, dot_ref, stage, flat, picked, packed, sem):
    n_ep, tok_rows, width = tok_ref.shape
    cap = list_ref.shape[2]
    sub = width // LANES
    load_table(table_ref, flat, stage, sem)

    def source(s, carry):
        take_rows(row_ref, s * cap, cap, sub, flat, picked, packed)
        full = lax.dot_general(tok_ref[s], packed[...], NT, preferred_element_type=jnp.float32)
        hit = hits(list_ref, s, tok_rows, table_ref.shape[0])
        dot_ref[s] = jnp.sum(jnp.where(hit, full, 0.0), axis=0, keepdims=True)
        return carry

    lax.fori_loop(0, n_ep, source, 0)


def mix_kernel(row_ref, list_ref, coef_ref, table_ref, mix_ref, stage, flat, picked, packed, sem):
    n_ep, tok_rows, width = mix_ref.shape
    cap = list_ref.shape[2]
    sub = width // LANES
    load_table(table_ref, flat, stage, sem)

    def source(s, carry):
        take_rows(row_ref, s * cap, cap, sub, flat, picked, packed)
        hit = hits(list_ref, s, tok_rows, table_ref.shape[0])
        coef = coef_ref[s]
        high = coef.astype(jnp.bfloat16).astype(jnp.float32)
        low = coef - high
        rows = packed[...]
        mixed = jnp.dot(jnp.where(hit, high, 0.0).astype(jnp.bfloat16), rows, preferred_element_type=jnp.float32)
        mixed += jnp.dot(jnp.where(hit, low, 0.0).astype(jnp.bfloat16), rows, preferred_element_type=jnp.float32)
        mix_ref[s] = mixed.astype(jnp.bfloat16)
        return carry

    lax.fori_loop(0, n_ep, source, 0)


def table_scratch(rows, width, cap):
    sub = width // LANES
    step = min(rows, 512)
    return [
        pltpu.VMEM((2, step, width), jnp.bfloat16),
        pltpu.VMEM((rows * sub, LANES), jnp.float32),
        pltpu.VMEM((cap * sub, LANES), jnp.float32),
        pltpu.VMEM((cap, width), jnp.bfloat16),
        pltpu.SemaphoreType.DMA((2,)),
    ]


def row_call(kernel, out, row_at, lists, middle, table, name):
    cap = lists.shape[2]
    vmem = pl.BlockSpec(memory_space=pltpu.VMEM)
    return pl.pallas_call(
        kernel,
        in_specs=[
            pl.BlockSpec(memory_space=pltpu.SMEM),
            vmem,
            vmem,
            pl.BlockSpec(memory_space=pl.ANY),
        ],
        out_specs=vmem,
        scratch_shapes=table_scratch(*table.shape, cap),
        out_shape=out,
        compiler_params=pltpu.CompilerParams(vmem_limit_bytes=VMEM_LIMIT),
        name=name,
    )(row_at, lists, middle, table)


def stage_layout(order, dims):
    bases, base = [], 0
    for j, dim in enumerate(order):
        bases.append(base)
        inner = int(np.prod([dims[order[i]] for i in range(j)]))
        base += (2 * dims[dim] if dims[dim] > 2 else 1) * inner
    return bases, base


def stage_slot(dims, order, bases, j, side, coords):
    n = dims[order[j]]
    inner, width = 0, 1
    for i in reversed(range(j)):
        inner = inner + coords[order[i]] * width
        width *= dims[order[i]]
    outer = (side * n + coords[order[j]]) if n > 2 else 0
    return bases[j] + outer * width + inner


def scatter_kernel(dims, plans, given_ref, out_ref, part_ref, *scratch):
    held = scratch[: len(plans)]
    rsems = scratch[len(plans) : 2 * len(plans)]
    ssem = scratch[-1]
    place = Place(dims)
    me = place.e
    barrier = pltpu.get_barrier_semaphore()
    around = []
    for dim, n in enumerate(dims):
        m = place.at[dim]
        if n == 2:
            around.append((place.moved(dim, 1 - m), None))
        else:
            around.append((place.moved(dim, m + 1), m + 1 < n))
            around.append((place.moved(dim, m - 1), m > 0))
    for to, pred in around:
        def greet(to=to):
            pl.semaphore_signal(barrier, inc=1, device_id=(to, place.tp), device_id_type=MESH)
        maybe(pred, greet)
    met = sum(1 if pred is None else jnp.where(pred, 1, 0) for _, pred in around)
    pl.semaphore_wait(barrier, met)

    load = pltpu.make_async_copy(given_ref, part_ref, scratch[-2])
    load.start()
    load.wait()
    layouts = [stage_layout(order, dims)[0] for order, _, _ in plans]
    sends = []

    def incoming(v, j, coords):
        order = plans[v][0]
        out = []
        for l, frm, pred in tree_neighbors(place, order, j, coords):
            dim = order[l]
            side = jnp.where(frm > place.at[dim], 1, 0)
            out.append((stage_slot(dims, order, layouts[v], l, side, coords), pred))
        out.sort(key=lambda t: t[1] is not None)
        return out

    def await_slot(v, slot):
        ref = held[v].at[slot]
        pltpu.make_async_remote_copy(
            src_ref=ref, dst_ref=ref, send_sem=ssem.at[0], recv_sem=rsems[v].at[slot],
            device_id=(me, place.tp), device_id_type=MESH,
        ).wait_recv()

    def add(v, d, slots, final):
        _, first, count = plans[v]
        unit = 16 if count % 16 == 0 else count

        def some(i, carry):
            r = pl.multiple_of(i * unit, unit)
            rows = pl.ds(first + r, unit)
            x = part_ref[d, rows, :].astype(jnp.float32)
            for slot in slots:
                x = x + held[v][slot, pl.ds(r, unit), :].astype(jnp.float32)
            if final:
                out_ref[rows, :] = x
            else:
                part_ref[d, rows, :] = x.astype(jnp.bfloat16)
            return carry

        lax.fori_loop(0, count // unit, some, 0)

    def collect(v, d, inc, final):
        sure = [slot for slot, pred in inc if pred is None]
        unsure = [(slot, pred) for slot, pred in inc if pred is not None]
        for slot in sure:
            await_slot(v, slot)
        for slot, pred in unsure:
            maybe(pred, functools.partial(await_slot, v, slot))
        if not unsure:
            if sure or final:
                add(v, d, sure, final)
            return
        for picks in itertools.product((True, False), repeat=len(unsure)):
            cond = None
            for (_, pred), yes in zip(unsure, picks):
                term = pred if yes else jnp.logical_not(pred)
                cond = term if cond is None else cond & term
            slots = sure + [slot for (slot, _), yes in zip(unsure, picks) if yes]
            if slots or final:
                maybe(cond, functools.partial(add, v, d, slots, final))

    for v, j, ks in reversed(schedule(plans, dims)):
        order, first, count = plans[v]
        coords = event_block(place, order, j, ks)
        d = place.flat(coords)
        collect(v, d, incoming(v, j, coords), False)
        dim = order[j]
        m = place.at[dim]
        to = 1 - m if dims[dim] == 2 else m + jnp.where(coords[dim] > m, 1, -1)
        side = jnp.where(m > to, 1, 0)
        slot = stage_slot(dims, order, layouts[v], j, side, coords)
        copy = pltpu.make_async_remote_copy(
            src_ref=part_ref.at[d, pl.ds(first, count)],
            dst_ref=held[v].at[slot],
            send_sem=ssem.at[len(sends)],
            recv_sem=rsems[v].at[slot],
            device_id=(place.moved(dim, to), place.tp),
            device_id_type=MESH,
        )
        copy.start()
        sends.append(copy)
    for v, (order, first, count) in enumerate(plans):
        collect(v, me, incoming(v, -1, place.at), True)
    for copy in sends:
        copy.wait_send()


def scatter_sum(part, dims, plans):
    n_ep, tok_rows, width = part.shape
    counts = [(stage_layout(order, dims)[1], count) for order, _, count in plans]
    vmem = pl.BlockSpec(memory_space=pltpu.VMEM)
    return pl.pallas_call(
        functools.partial(scatter_kernel, dims, plans),
        out_shape=jax.ShapeDtypeStruct((tok_rows, width), jnp.float32),
        in_specs=[pl.BlockSpec(memory_space=pl.ANY)],
        out_specs=vmem,
        scratch_shapes=[pltpu.VMEM(part.shape, jnp.bfloat16)]
        + [pltpu.VMEM((slots, count, width), jnp.bfloat16) for slots, count in counts]
        + [pltpu.SemaphoreType.DMA((slots,)) for slots, _ in counts]
        + [pltpu.SemaphoreType.DMA, pltpu.SemaphoreType.DMA((len(schedule(plans, dims)),))],
        compiler_params=pltpu.CompilerParams(
            collective_id=1, has_side_effects=True, vmem_limit_bytes=VMEM_LIMIT
        ),
        name="scatter_sum",
    )(part)


def body(dims, tokens, experts, weights, up_table, out_table, gain):
    n_ep = lax.axis_size("ep")
    tok_rows, width = tokens.shape
    slots = experts.shape[1]
    rows_held = up_table.shape[0]
    sub = width // LANES
    cap = 2 * tok_rows * slots // n_ep
    plans = tree_plans(dims, tok_rows)
    lists = route(experts.T, weights.T, n_ep, cap, rows_held)
    tok_all, lists_all = gather_tokens(tokens, lists, dims, plans)
    row_at = ((lists_all[:, 0, :].astype(jnp.int32) % rows_held) * sub).reshape(-1)
    dot_shape = jax.ShapeDtypeStruct((n_ep, 1, cap), jnp.float32)
    partial_dot = row_call(dots_kernel, dot_shape, row_at, lists_all, tok_all, up_table, "request_dots")
    dot = lax.psum(partial_dot, "tp")
    coef = lists_all[:, 1:2, :] * jax.nn.gelu(dot)
    part_shape = jax.ShapeDtypeStruct((n_ep, tok_rows, width), jnp.bfloat16)
    part = row_call(mix_kernel, part_shape, row_at, lists_all, coef, out_table, "mix_rows")
    mixed = scatter_sum(part, dims, plans)
    square = lax.psum(jnp.sum(mixed * mixed, axis=1), "tp")
    scale = lax.rsqrt(square / (width * lax.axis_size("tp")) + 1e-06)
    return (mixed * scale[:, None] * gain[None, :]).astype(jnp.bfloat16)


def solution(mesh):
    placed = (P("ep", "tp"), P("ep", None), P("ep", None), P("ep", "tp"), P("ep", "tp"), P("tp"))
    return jax.shard_map(
        functools.partial(body, ep_dims(mesh)), mesh=mesh, in_specs=placed, out_specs=P("ep", "tp"), check_vma=False
    )
```

time: 400 us -> 247 us (0.62); the launches traced: 395 us -> 246 us
  waiting for transfers between devices: 222 us -> 0 us
  Pallas kernels: 76.6 us -> 231 us
  local copies, waits for them, and re-layouts: 54.7 us -> 0.01 us
  between operations: 13.5 us -> 0.06 us
  starting transfers between devices: 13.1 us -> 0 us
    reduce_scatter x1 -> x0, waiting for transfers between devices: 176 us -> none  [body(): lax.psum_scatter(part, 'ep', scatter_dimension=0, tiled=True)]
    pallas_call x2 -> x5, Pallas kernels: 76.6 us -> 231 us  [the longest x1 76.1 us: scatter_sum(): pl.pallas_call(functools.partial(scatter_kernel, dims, plans), out_shape=...]
    all_gather x1 -> x0, waiting for transfers between devices: 46.1 us -> none  [body(): lax.all_gather(tokens.reshape(tok_rows, sub, LANES), 'ep', axis=0, tiled=...]
    scatter x2 -> x0, local copies, waits for them, and re-layouts: 32.2 us -> none  [the longest x1 16.1 us: body(): send_words = jnp.zeros((n_ep * capacity,), jnp.int32).at[position].set(to...]
    unnamed x11 -> x4, local copies, waits for them, and re-layouts: 22.2 us -> 0.01 us
    all_to_all x2 -> x0, starting transfers between devices: 13 us -> none  [the longest x1 6.66 us: body(): lax.all_to_all(send_words.reshape(n_ep, capacity), 'ep', 0, 0, tiled=True)]
  transfers between devices with their start and end apart: 4 -> 0, of which waited for: 2 -> 0; matrix products, arithmetic and copies ran while one was open for 13% -> 0% of each run, Pallas kernels for 9% -> 0%
where the time goes in v1:
time: 247 us; the launch traced here: 246 us
  Pallas kernels  231 us (94%)
  blocking collectives  10 us (4%)
  other arithmetic  5.77 us (2%)
    pallas_call x1, Pallas kernels, scatter_sum(): pl.pallas_call(functools.partial(scatter_kernel, dims, plans), out_shape=...  76.1 us
    pallas_call x1, Pallas kernels, gather_tokens(): pl.pallas_call(functools.partial(gather_kernel, dims, plans), out_shape=(...  75.2 us
    pallas_call x2, Pallas kernels, row_call(): pl.pallas_call(kernel, in_specs=[pl.BlockSpec(memory_space=pltpu.SMEM), v...  74.1 us
    psum x1, blocking collectives, body(): dot = lax.psum(partial_dot, 'tp')  5.67 us
    pallas_call x1, Pallas kernels, route(): pl.pallas_call(functools.partial(route_kernel, n_ep, cap, rows_held), out...  5.21 us

profile of v1, /device:TPU:9, one launch (start us, length us, event | category | flops | bytes accessed | tf_op | source)
XLA Modules:
  0.0 246.4 jit_solution(9124952402987414401)
XLA Ops:
  0.0 5.2 %route.1.list_ref = f32[16,2,512]{2,1,0:T(2,128)} custom-call(s32[16,256]{1,0:T(8,128)} %bitcast.4, f32[16,256]{1,0:T(8,128)} %bitcast.5), custom_call_target="tpu_custom_call" | custom-call | tf_op jit(solution)/shard_map/route/pallas_call | solution.py:181
  5.2 75.2 %gather_tokens.1 = (bf16[16,256,1024]{2,1,0:T(8,128)(2,1)}, f32[16,2,512]{2,1,0:T(2,128)}) custom-call(bf16[256,1024]{1,0:T(8,128)(2,1)} %tok_ref.1, f32[16,2,512]{2,1,0:T(2,128)} %route.1.list_ref), custom_call_target="tpu_custom_call" | custom-call | tf_op jit(solution)/shard_map/gather_tokens/pallas_call | solution.py:266
  80.4 0.9 slice_convert_fusion
  81.3 0.6 fusion.1.row_ref
  81.9 0.0 copy-start
  81.9 34.3 %request_dots.1 = f32[16,1,512]{2,1,0:T(1,128)} custom-call(s32[8192]{0:T(1024)} %fusion.1.row_ref, f32[16,2,512]{2,1,0:T(2,128)} %get-tuple-element.7.list_ref, bf16[16,256,1024]{2,1,0:T(8,128)(2,1)} %get-tuple-element.8.tok_ref, bf16[4096,1024]{1,0:T(8,128)(2,1)} %table_ref.2), custom_call_target="tpu_custom_call" | custom-call | tf_op jit(solution)/shard_map/request_dots/pallas_call | solution.py:389
  116.2 5.7 %psum.14 = f32[16,1,512]{2,1,0:T(1,128)S(1)} all-reduce(f32[16,1,512]{2,1,0:T(1,128)} %request_dots.1), channel_id=1, replica_groups=mesh['ep'=16,'tp'=2] {'tp'}, use_global_device_ids=true, to_apply=%region_0.1 | all-reduce | flops 8192 | bytes 65536 | tf_op jit(solution)/shard_map/psum | solution.py:566
  121.9 0.0 copy-done
  121.9 0.7 fusion.9.coef_ref
  122.6 39.8 %mix_rows.1.given_ref = bf16[16,256,1024]{2,1,0:T(8,128)(2,1)} custom-call(s32[8192]{0:T(1024)} %fusion.1.row_ref, f32[16,2,512]{2,1,0:T(2,128)} %get-tuple-element.7.list_ref, f32[16,1,512]{2,1,0:T(1,128)} %fusion.9.coef_ref, bf16[4096,1024]{1,0:T(8,128)(2,1)} %table_ref.3), custom_call_target="tpu_custom_call" | custom-call | tf_op jit(solution)/shard_map/mix_rows/pallas_call | solution.py:389
  162.4 0.0 copy-start.1
  162.4 76.1 %scatter_sum.1 = f32[256,1024]{1,0:T(8,128)} custom-call(bf16[16,256,1024]{2,1,0:T(8,128)(2,1)} %mix_rows.1.given_ref), custom_call_target="tpu_custom_call" | custom-call | tf_op jit(solution)/shard_map/scatter_sum/pallas_call | solution.py:537
  238.5 1.4 multiply_reduce_fusion
  239.9 4.4 %psum.15 = f32[256]{0:T(256)S(1)} all-reduce(f32[256]{0:T(256)S(1)} %multiply_reduce_fusion), channel_id=1, replica_groups=mesh['ep'=16,'tp'=2] {'tp'}, use_global_device_ids=true, to_apply=%region_2.3 | all-reduce | flops 256 | bytes 2048 | tf_op jit(solution)/shard_map/psum | solution.py:571
  244.3 0.0 copy-done.1
  244.3 2.2 multiply_convert_fusion
  (1 shorter events, 0.0 us)
Async XLA Ops:
  81.9 40.0 %copy-start = (f32[16,2,512]{2,1,0:T(2,128)S(1)}, f32[16,2,512]{2,1,0:T(2,128)}, u32[]{:S(2)}) copy-start(f32[16,2,512]{2,1,0:T(2,128)} %get-tuple-element.7.list_ref) | copy-start | bytes 196612
  162.4 81.9 %copy-start.1 = (f32[1024]{0:T(1024)S(1)}, f32[1024]{0:T(1024)}, u32[]{:S(2)}) copy-start(f32[1024]{0:T(1024)} %param.11) | copy-start | bytes 12292

commit v2 on v1

v2 whole, which is shorter than its diff:
```python
import functools
import itertools

import jax
import jax.numpy as jnp
import numpy as np
from jax import lax
from jax.experimental import pallas as pl
from jax.experimental.pallas import tpu as pltpu
from jax.sharding import PartitionSpec as P

LANES = 128
MESH = pl.DeviceIdType.MESH
NT = (((1,), (1,)), ((), ()))
VMEM_LIMIT = 63 * 1024 * 1024
PITCH = 9
DEPTH = 8
SCATTER_ORDER = ()
GATHER_ORDER = (
    0, 15, 1, 31, 30, 46, 45, 18, 48, 3, 49, 19, 16, 5, 36, 7, 11, 37, 51, 54, 47, 4, 32, 52, 33, 55,
    50, 39, 34, 20, 2, 17, 58, 42, 22, 25, 40, 57, 43, 6, 35, 41, 9, 12, 24, 53, 28, 21, 13, 26, 10, 44,
    59, 56, 8, 38, 27, 14, 23, 29,
)


def ep_dims(mesh):
    n = mesh.shape["ep"]
    devices = np.moveaxis(mesh.devices, mesh.axis_names.index("ep"), 0).reshape(n, -1)[:, 0]
    coords = [getattr(d, "coords", None) for d in devices]
    if any(c is None for c in coords):
        return (n,)
    axes = []
    for a in range(len(coords[0])):
        values = [c[a] for c in coords]
        size = len(set(values))
        if size > 1:
            stride = next(i for i in range(n) if values[i] != values[0])
            axes.append((stride, size, [v - min(values) for v in values]))
    axes.sort(key=lambda t: -t[0])
    dims = tuple(size for _, size, _ in axes)
    if int(np.prod(dims)) != n:
        return (n,)
    for i in range(n):
        if any((i // stride) % size != values[i] for stride, size, values in axes):
            return (n,)
    return dims


def tree_plans(dims, rows):
    k = len(dims)
    if k == 3 and rows % 128 == 0:
        long, mid, last = sorted(range(3), key=lambda i: -dims[i])
        unit = rows // 8
        plans = [
            ((long, mid, last), 3 * unit),
            ((long, last, mid), 3 * unit),
            ((last, mid, long), unit),
            ((mid, last, long), unit),
        ]
    elif k == 2 and rows % 32 == 0:
        plans = [((0, 1), rows // 2), ((1, 0), rows // 2)]
    else:
        plans = [(tuple(range(k)), rows)]
    out, first = [], 0
    for order, count in plans:
        out.append((order, first, count))
        first += count
    return out


class Place:
    def __init__(self, dims):
        self.dims = dims
        self.strides = [int(np.prod(dims[i + 1 :])) for i in range(len(dims))]
        self.e = lax.axis_index("ep")
        self.tp = lax.axis_index("tp")
        self.at = [(self.e // st) % n for st, n in zip(self.strides, dims)]

    def near(self, dim, k):
        m, n = self.at[dim], self.dims[dim]
        if k == 0:
            return m
        if n == 2:
            return 1 - m
        below, above = m, n - 1 - m
        low = jnp.minimum(below, above)
        hop = (k + 1) // 2
        alternate = m + hop if k % 2 else m - hop
        far = jnp.where(below < above, m + (k - low), m - (k - low))
        return jnp.where(k <= 2 * low, alternate, far)

    def flat(self, coords):
        total = 0
        for c, st in zip(coords, self.strides):
            total = total + c * st
        return total

    def moved(self, dim, to):
        return self.e + (to - self.at[dim]) * self.strides[dim]


def tree_events(order, dims):
    events = []
    for j in range(len(order)):
        heads = [range(dims[order[i]]) for i in range(j)] + [range(1, dims[order[j]])]
        for ks in itertools.product(*heads):
            events.append((j, ks))
    return events


def event_block(place, order, j, ks):
    coords = list(place.at)
    for i in range(j + 1):
        coords[order[i]] = place.near(order[i], ks[i])
    return coords


def tree_neighbors(place, order, j, coords):
    out = []
    for l in range(max(j, 0), len(order)):
        dim = order[l]
        n, m = place.dims[dim], place.at[dim]
        if l == j:
            if n > 2:
                to = m + jnp.where(m > coords[dim], 1, -1)
                out.append((l, to, (to >= 0) & (to < n)))
        elif n == 2:
            out.append((l, 1 - m, None))
        else:
            out.append((l, m + 1, m + 1 < n))
            out.append((l, m - 1, m > 0))
    return out


def schedule(plans, dims, table):
    keyed = []
    for v, (order, _, count) in enumerate(plans):
        seen = {}
        for j, ks in tree_events(order, dims):
            dist = sum((k + 1) // 2 if dims[order[i]] > 2 else k for i, k in enumerate(ks))
            before = seen.get(j, 0)
            seen[j] = before + 1
            keyed.append(((dist + before) * 1.0 + 0.01 * j, v, j, ks))
    events = [(v, j, ks) for _, v, j, ks in keyed]
    if len(events) == len(table):
        return [events[i] for i in table]
    keyed.sort(key=lambda t: t[0])
    return [(v, j, ks) for _, v, j, ks in keyed]


def relative(plans, v, ks):
    order = plans[v][0]
    ranks = [0] * len(order)
    for i, k in enumerate(ks):
        ranks[order[i]] = k
    return tuple(ranks)


def block_of(place, ranks):
    return place.flat([place.near(dim, k) for dim, k in enumerate(ranks)])


def maybe(pred, fn):
    if pred is None:
        fn()
    else:
        pl.when(pred)(fn)


def count_sends(plans, dims):
    total = 0
    for order, _, _ in plans:
        for j, _ in [(-1, ())] + tree_events(order, dims):
            for l in range(max(j, 0), len(order)):
                big = dims[order[l]] > 2
                total += (1 if big else 0) if l == j else (2 if big else 1)
    return total


def route_kernel(n_ep, cap, rows_held, sub, experts_ref, weights_ref, word_ref, weight_ref):
    slots, tok_rows = experts_ref.shape
    col = lax.broadcasted_iota(jnp.int32, (tok_rows, tok_rows), 1)
    row = lax.broadcasted_iota(jnp.int32, (tok_rows, tok_rows), 0)
    before = (row < col).astype(jnp.float32).astype(jnp.bfloat16)
    owners = lax.broadcasted_iota(jnp.int32, (n_ep, tok_rows), 0)
    places = lax.broadcasted_iota(jnp.int32, (cap, tok_rows), 0)
    token = lax.broadcasted_iota(jnp.int32, (1, tok_rows), 1)
    base = jnp.zeros((n_ep, 1), jnp.float32)
    total = jnp.zeros((6 * n_ep, cap), jnp.float32)
    for k in range(slots):
        e = experts_ref[k : k + 1, :]
        owner = e // rows_held
        mine = owner == owners
        ones = jnp.where(mine, 1.0, 0.0)
        ahead = jnp.dot(ones.astype(jnp.bfloat16), before, preferred_element_type=jnp.float32) + base
        base = base + jnp.sum(ones, axis=1, keepdims=True)
        rank = jnp.sum(jnp.where(mine, ahead, 0.0), axis=0, keepdims=True).astype(jnp.int32)
        at = jnp.where(rank == places, 1.0, 0.0).astype(jnp.bfloat16)
        word = token * rows_held + (e - owner * rows_held)
        w = weights_ref[k : k + 1, :]
        w0 = w.astype(jnp.bfloat16).astype(jnp.float32)
        w1 = (w - w0).astype(jnp.bfloat16).astype(jnp.float32)
        w2 = w - w0 - w1
        parts = [(word & 255), ((word >> 8) & 255), (word >> 16)]
        parts = [p.astype(jnp.float32) for p in parts] + [w0, w1, w2]
        lhs = jnp.concatenate([jnp.where(mine, p, 0.0) for p in parts], axis=0).astype(jnp.bfloat16)
        total = total + lax.dot_general(lhs, at, NT, preferred_element_type=jnp.float32)
    take = lambda i: total[i * n_ep : (i + 1) * n_ep, :]
    word = (take(0) + 256.0 * take(1) + 65536.0 * take(2)).astype(jnp.int32)
    token = word // rows_held
    row = word - token * rows_held
    line = (row // 8) * (sub * PITCH - 8) + row
    word_ref[:, 0, :] = token * lines_of(rows_held, sub) + line
    weight_ref[:, 0, :] = take(3) + take(4) + take(5)


def lines_of(rows_held, sub):
    return rows_held // 8 * sub * PITCH


def route(experts_t, weights_t, n_ep, cap, rows_held, sub):
    lists = (n_ep, 1, cap)
    return pl.pallas_call(
        functools.partial(route_kernel, n_ep, cap, rows_held, sub),
        out_shape=(jax.ShapeDtypeStruct(lists, jnp.int32), jax.ShapeDtypeStruct(lists, jnp.float32)),
        name="route",
    )(experts_t, weights_t)


def table_piece(table_ref, flat, stage, sem, i, slot):
    step, width = stage.shape[1:]
    sub = width // LANES
    copy = pltpu.make_async_copy(table_ref.at[pl.ds(i * step, step)], stage.at[slot], sem.at[slot])

    def rest():
        copy.wait()

        def spread(g, carry):
            r = pl.multiple_of(g * 16, 16)
            for c in range(sub):
                x = stage[slot, pl.ds(r, 16), c * LANES : (c + 1) * LANES].astype(jnp.float32)
                for h in range(2):
                    first = ((i * (step // 8) + g * 2 + h) * sub + c) * PITCH
                    flat[pl.ds(first, 8), :] = x[8 * h : 8 * h + 8, :]
            return carry

        lax.fori_loop(0, step // 16, spread, 0)

    return copy.start, rest


def take_rows(row_ref, s, sub, flat, picked, put):
    cap = row_ref.shape[1]
    unroll = 32
    gap = sub + 1 if sub > 1 else 1

    def some(g, carry):
        taken = []
        for u in range(unroll):
            at = row_ref[s, g * unroll + u]
            taken.append(flat[pl.ds(at, sub, stride=PITCH), :] if sub > 1 else flat[pl.ds(at, 1), :])
        for u in range(unroll):
            picked[pl.ds((g * unroll + u) * gap, sub), :] = taken[u]
        return carry

    lax.fori_loop(0, cap // unroll, some, 0)
    for c in range(sub):
        lines = picked[pl.ds(c, cap, stride=gap), :] if sub > 1 else picked[...]
        put(c, lines.astype(jnp.bfloat16))


def collect_kernel(
    dims, plans, n_tp, my_word, my_weight, tok_ref, up_ref, out_ref,
    coef_ref, word_ref, rows_ref,
    all_ref, weight_ref, row_held, row_ref, stage, flat, picked, packed, held, dots, others,
    ssem, rsem, wssem, wrsem, ossem, orsem, stage_sem, put_sem, row_sem,
):
    place = Place(dims)
    me = place.e
    n_ep, tok_rows, width = all_ref.shape
    cap = coef_ref.shape[2]
    rows_held = up_ref.shape[0]
    sub = width // LANES
    lines = lines_of(rows_held, sub)
    pieces = rows_held // stage.shape[1]
    depth = min(stage.shape[0], pieces)
    loads = [
        table_piece(table, flat, stage, stage_sem, i, i % depth) for table in (out_ref, up_ref) for i in range(pieces)
    ]
    for i in range(depth):
        loads[i][0]()

    barrier = pltpu.get_barrier_semaphore()
    for o in range(1, n_ep):
        pl.semaphore_signal(barrier, inc=1, device_id=((me + o) % n_ep, place.tp), device_id_type=MESH)
    for o in range(1, n_tp):
        pl.semaphore_signal(barrier, inc=1, device_id=(me, (place.tp + o) % n_tp), device_id_type=MESH)
    pl.semaphore_wait(barrier, n_ep + n_tp - 2)

    sends = []

    def forward(v, j, coords, src):
        order, first, count = plans[v]
        s = place.flat(coords)
        for l, to, pred in tree_neighbors(place, order, j, coords):
            copy = pltpu.make_async_remote_copy(
                src_ref=src,
                dst_ref=all_ref.at[s, pl.ds(first, count)],
                send_sem=ssem.at[len(sends)],
                recv_sem=rsem.at[v, s],
                device_id=(place.moved(order[l], to), place.tp),
                device_id_type=MESH,
            )
            maybe(pred, copy.start)
            sends.append((pred, copy))

    list_copies = []
    for o in range(1, n_ep):
        to = (me + o) % n_ep
        for i, (src, dst) in enumerate(((my_word, word_ref), (my_weight, weight_ref))):
            copy = pltpu.make_async_remote_copy(
                src_ref=src.at[to],
                dst_ref=dst.at[me],
                send_sem=wssem.at[i, o],
                recv_sem=wrsem.at[i, o],
                device_id=(to, place.tp),
                device_id_type=MESH,
            )
            copy.start()
            list_copies.append(copy)
    for v, (order, first, count) in enumerate(plans):
        forward(v, -1, place.at, tok_ref.at[pl.ds(first, count)])
    word_ref[me] = my_word[me]
    weight_ref[me] = my_weight[me]

    def load(i):
        loads[i][1]()
        if i + depth < len(loads):
            loads[i + depth][0]()

    def lists():
        for copy in list_copies:
            copy.wait_recv()
        for s in range(n_ep):
            word = word_ref[s]
            row_held[s : s + 1, :] = word - (word // lines) * lines
        copy = pltpu.make_async_copy(row_held, row_ref, row_sem)
        copy.start()
        copy.wait()

    def put_copy(s):
        return pltpu.make_async_copy(packed.at[s % 2], rows_ref.at[s], put_sem.at[s % 2])

    def out_rows(s):
        if s >= 2:
            put_copy(s - 2).wait()

        def put(c, lines):
            packed[s % 2, :, c * LANES : (c + 1) * LANES] = lines

        take_rows(row_ref, s, sub, flat, picked, put)
        put_copy(s).start()

    def up_rows(s):
        def put(c, lines):
            held[s, :, c * LANES : (c + 1) * LANES] = lines

        take_rows(row_ref, s, sub, flat, picked, put)

    def dot_of(ranks):
        s = block_of(place, ranks)
        tok = tok_ref[...] if not any(ranks) else all_ref[s]
        full = lax.dot_general(tok, held[s], NT, preferred_element_type=jnp.float32)
        hit = (word_ref[s] // lines) == lax.broadcasted_iota(jnp.int32, (tok_rows, cap), 0)
        dots[s] = jnp.sum(jnp.where(hit, full, 0.0), axis=0, keepdims=True)

    events = schedule(plans, dims, GATHER_ORDER)
    last = {}
    for i, (v, j, ks) in enumerate(events):
        last[relative(plans, v, ks)] = i
    work = [(0.3, functools.partial(load, i)) for i in range(pieces)] + [(0.5, lists)]
    work += [(0.8, functools.partial(out_rows, s)) for s in range(n_ep)]
    work += [(0.3, functools.partial(load, pieces + i)) for i in range(pieces)]
    work += [(0.8, functools.partial(up_rows, s)) for s in range(n_ep)]
    ready = [(0,) * len(dims)]
    clock, per_event = 3.0, 62.0 / len(events)
    for i, (v, j, ks) in enumerate(events):
        due = 4.0 + per_event * i
        while clock < due and (work or ready):
            if work:
                cost, fn = work.pop(0)
                fn()
                clock += cost
            else:
                dot_of(ready.pop(0))
                clock += 0.5
        clock = max(clock, due)
        order, first, count = plans[v]
        coords = event_block(place, order, j, ks)
        s = place.flat(coords)
        block = all_ref.at[s, pl.ds(first, count)]
        pltpu.make_async_remote_copy(
            src_ref=block, dst_ref=block, send_sem=ssem.at[0], recv_sem=rsem.at[v, s],
            device_id=(me, place.tp), device_id_type=MESH,
        ).wait_recv()
        forward(v, j, coords, block)
        ranks = relative(plans, v, ks)
        if last[ranks] == i:
            ready.append(ranks)
    for _, fn in work:
        fn()
    for ranks in ready:
        dot_of(ranks)

    shares = []
    for o in range(1, n_tp):
        copy = pltpu.make_async_remote_copy(
            src_ref=dots,
            dst_ref=others.at[o],
            send_sem=ossem.at[o],
            recv_sem=orsem.at[o],
            device_id=(me, (place.tp + o) % n_tp),
            device_id_type=MESH,
        )
        copy.start()
        shares.append(copy)
    for copy in shares:
        copy.wait_recv()

    def finish(s, carry):
        dot = dots[s]
        for o in range(1, n_tp):
            dot = dot + others[o, s]
        coef_ref[s] = weight_ref[s] * jax.nn.gelu(dot)
        return carry

    lax.fori_loop(0, n_ep, finish, 0)
    for copy in shares + list_copies:
        copy.wait_send()
    for s in range(max(0, n_ep - 2), n_ep):
        put_copy(s).wait()
    for pred, copy in sends:
        maybe(pred, copy.wait_send)


def collect(words, weights, tokens, up_table, out_table, dims, plans, n_tp, cap):
    n_ep = int(np.prod(dims))
    tok_rows, width = tokens.shape
    rows_held = up_table.shape[0]
    sub = width // LANES
    vmem = pl.BlockSpec(memory_space=pltpu.VMEM)
    hbm = pl.BlockSpec(memory_space=pl.ANY)
    lists = (n_ep, 1, cap)
    return pl.pallas_call(
        functools.partial(collect_kernel, dims, plans, n_tp),
        out_shape=(
            jax.ShapeDtypeStruct(lists, jnp.float32),
            jax.ShapeDtypeStruct(lists, jnp.int32),
            jax.ShapeDtypeStruct((n_ep, cap, width), jnp.bfloat16),
        ),
        in_specs=[vmem, vmem, vmem, hbm, hbm],
        out_specs=(vmem, vmem, hbm),
        scratch_shapes=[
            pltpu.VMEM((n_ep, tok_rows, width), jnp.bfloat16),
            pltpu.VMEM(lists, jnp.float32),
            pltpu.VMEM((n_ep, cap), jnp.int32),
            pltpu.SMEM((n_ep, cap), jnp.int32),
            pltpu.VMEM((DEPTH, min(rows_held, 256), width), jnp.bfloat16),
            pltpu.VMEM((lines_of(rows_held, sub), LANES), jnp.float32),
            pltpu.VMEM((cap * (sub + 1 if sub > 1 else 1), LANES), jnp.float32),
            pltpu.VMEM((2, cap, width), jnp.bfloat16),
            pltpu.VMEM((n_ep, cap, width), jnp.bfloat16),
            pltpu.VMEM(lists, jnp.float32),
            pltpu.VMEM((n_tp,) + lists, jnp.float32),
            pltpu.SemaphoreType.DMA((count_sends(plans, dims),)),
            pltpu.SemaphoreType.DMA((len(plans), n_ep)),
            pltpu.SemaphoreType.DMA((2, n_ep)),
            pltpu.SemaphoreType.DMA((2, n_ep)),
            pltpu.SemaphoreType.DMA((n_tp,)),
            pltpu.SemaphoreType.DMA((n_tp,)),
            pltpu.SemaphoreType.DMA((DEPTH,)),
            pltpu.SemaphoreType.DMA((2,)),
            pltpu.SemaphoreType.DMA,
        ],
        compiler_params=pltpu.CompilerParams(
            collective_id=0, has_side_effects=True, vmem_limit_bytes=VMEM_LIMIT
        ),
        name="collect",
    )(words, weights, tokens, up_table, out_table)


def stage_layout(order, dims):
    bases, base = [], 0
    for j, dim in enumerate(order):
        bases.append(base)
        inner = int(np.prod([dims[order[i]] for i in range(j)]))
        base += (2 * dims[dim] if dims[dim] > 2 else 1) * inner
    return bases, base


def stage_slot(dims, order, bases, j, side, coords):
    n = dims[order[j]]
    inner, width = 0, 1
    for i in reversed(range(j)):
        inner = inner + coords[order[i]] * width
        width *= dims[order[i]]
    outer = (side * n + coords[order[j]]) if n > 2 else 0
    return bases[j] + outer * width + inner


def scatter_kernel(dims, plans, n_tp, lines, coef_ref, word_ref, gain_ref, rows_ref, out_ref, part_ref, mixed, squares, others, rows, *scratch):
    held = scratch[: len(plans)]
    rsems = scratch[len(plans) : 2 * len(plans)]
    row_sem, ossem, orsem, ssem = scratch[-4:]
    place = Place(dims)
    me = place.e
    n_ep, tok_rows, width = part_ref.shape
    cap = coef_ref.shape[2]
    events = list(reversed(schedule(plans, dims, SCATTER_ORDER)))
    needed = []
    for v, j, ks in events:
        ranks = relative(plans, v, ks)
        if ranks not in needed:
            needed.append(ranks)
    needed.append((0,) * len(dims))
    depth = rows.shape[0]

    def fetch(i):
        return pltpu.make_async_copy(rows_ref.at[block_of(place, needed[i])], rows.at[i % depth], row_sem.at[i % depth])

    for i in range(min(depth, n_ep)):
        fetch(i).start()
    barrier = pltpu.get_barrier_semaphore()
    around = []
    for dim, n in enumerate(dims):
        m = place.at[dim]
        if n == 2:
            around.append((place.moved(dim, 1 - m), None))
        else:
            around.append((place.moved(dim, m + 1), m + 1 < n))
            around.append((place.moved(dim, m - 1), m > 0))
    for to, pred in around:
        def greet(to=to):
            pl.semaphore_signal(barrier, inc=1, device_id=(to, place.tp), device_id_type=MESH)
        maybe(pred, greet)
    for o in range(1, n_tp):
        pl.semaphore_signal(barrier, inc=1, device_id=(me, (place.tp + o) % n_tp), device_id_type=MESH)
    met = sum(1 if pred is None else jnp.where(pred, 1, 0) for _, pred in around)
    pl.semaphore_wait(barrier, met + n_tp - 1)

    layouts = [stage_layout(order, dims)[0] for order, _, _ in plans]
    sends = []

    def mix(i):
        d = block_of(place, needed[i])
        fetch(i).wait()
        hit = (word_ref[d] // lines) == lax.broadcasted_iota(jnp.int32, (tok_rows, cap), 0)
        coef = coef_ref[d]
        high = coef.astype(jnp.bfloat16).astype(jnp.float32)
        low = coef - high
        table_rows = rows[i % depth]
        total = jnp.dot(jnp.where(hit, high, 0.0).astype(jnp.bfloat16), table_rows, preferred_element_type=jnp.float32)
        total += jnp.dot(jnp.where(hit, low, 0.0).astype(jnp.bfloat16), table_rows, preferred_element_type=jnp.float32)
        part_ref[d] = total.astype(jnp.bfloat16)
        if i + depth < n_ep:
            fetch(i + depth).start()

    def incoming(v, j, coords):
        order = plans[v][0]
        out = []
        for l, frm, pred in tree_neighbors(place, order, j, coords):
            dim = order[l]
            side = jnp.where(frm > place.at[dim], 1, 0)
            out.append((stage_slot(dims, order, layouts[v], l, side, coords), pred))
        out.sort(key=lambda t: t[1] is not None)
        return out

    def await_slot(v, slot):
        ref = held[v].at[slot]
        pltpu.make_async_remote_copy(
            src_ref=ref, dst_ref=ref, send_sem=ssem.at[0], recv_sem=rsems[v].at[slot],
            device_id=(me, place.tp), device_id_type=MESH,
        ).wait_recv()

    def add(v, d, slots, final):
        _, first, count = plans[v]
        unit = 16 if count % 16 == 0 else count

        def some(i, carry):
            r = pl.multiple_of(i * unit, unit)
            at = pl.ds(first + r, unit)
            x = part_ref[d, at, :].astype(jnp.float32)
            for slot in slots:
                x = x + held[v][slot, pl.ds(r, unit), :].astype(jnp.float32)
            if final:
                mixed[at, :] = x
                y = x * x
                square = y[:, :LANES]
                for c in range(1, width // LANES):
                    square = square + y[:, c * LANES : (c + 1) * LANES]
                squares[at, :] = square
            else:
                part_ref[d, at, :] = x.astype(jnp.bfloat16)
            return carry

        lax.fori_loop(0, count // unit, some, 0)

    def collect_parts(v, d, inc, final):
        sure = [slot for slot, pred in inc if pred is None]
        unsure = [(slot, pred) for slot, pred in inc if pred is not None]
        for slot in sure:
            await_slot(v, slot)
        for slot, pred in unsure:
            maybe(pred, functools.partial(await_slot, v, slot))
        if not unsure:
            if sure or final:
                add(v, d, sure, final)
            return
        for picks in itertools.product((True, False), repeat=len(unsure)):
            cond = None
            for (_, pred), yes in zip(unsure, picks):
                term = pred if yes else jnp.logical_not(pred)
                cond = term if cond is None else cond & term
            slots = sure + [slot for (slot, _), yes in zip(unsure, picks) if yes]
            if slots or final:
                maybe(cond, functools.partial(add, v, d, slots, final))

    done = 0
    for v, j, ks in events:
        order, first, count = plans[v]
        coords = event_block(place, order, j, ks)
        d = place.flat(coords)
        while relative(plans, v, ks) not in needed[:done]:
            mix(done)
            done += 1
        collect_parts(v, d, incoming(v, j, coords), False)
        dim = order[j]
        m = place.at[dim]
        to = 1 - m if dims[dim] == 2 else m + jnp.where(coords[dim] > m, 1, -1)
        side = jnp.where(m > to, 1, 0)
        slot = stage_slot(dims, order, layouts[v], j, side, coords)
        copy = pltpu.make_async_remote_copy(
            src_ref=part_ref.at[d, pl.ds(first, count)],
            dst_ref=held[v].at[slot],
            send_sem=ssem.at[len(sends)],
            recv_sem=rsems[v].at[slot],
            device_id=(place.moved(dim, to), place.tp),
            device_id_type=MESH,
        )
        copy.start()
        sends.append(copy)
    while done < n_ep:
        mix(done)
        done += 1
    for v, (order, first, count) in enumerate(plans):
        collect_parts(v, me, incoming(v, -1, place.at), True)

    shares = []
    for o in range(1, n_tp):
        copy = pltpu.make_async_remote_copy(
            src_ref=squares,
            dst_ref=others.at[o],
            send_sem=ossem.at[o],
            recv_sem=orsem.at[o],
            device_id=(me, (place.tp + o) % n_tp),
            device_id_type=MESH,
        )
        copy.start()
        shares.append(copy)
    for copy in shares:
        copy.wait_recv()
    unit = 32

    def norm(i, carry):
        at = pl.ds(pl.multiple_of(i * unit, unit), unit)
        square = squares[at, :]
        for o in range(1, n_tp):
            square = square + others[o, at, :]
        power = jnp.sum(square, axis=1, keepdims=True) / (width * n_tp)
        out_ref[at, :] = (mixed[at, :] * lax.rsqrt(power + 1e-06) * gain_ref[...]).astype(jnp.bfloat16)
        return carry

    lax.fori_loop(0, tok_rows // unit, norm, 0)
    for copy in shares + sends:
        copy.wait_send()


def scatter_norm(coef, words, gain, rows, dims, plans, n_tp, tok_rows, lines):
    n_ep, cap, width = rows.shape
    counts = [(stage_layout(order, dims)[1], count) for order, _, count in plans]
    vmem = pl.BlockSpec(memory_space=pltpu.VMEM)
    depth = 3
    return pl.pallas_call(
        functools.partial(scatter_kernel, dims, plans, n_tp, lines),
        out_shape=jax.ShapeDtypeStruct((tok_rows, width), jnp.bfloat16),
        in_specs=[vmem, vmem, vmem, pl.BlockSpec(memory_space=pl.ANY)],
        out_specs=vmem,
        scratch_shapes=[
            pltpu.VMEM((n_ep, tok_rows, width), jnp.bfloat16),
            pltpu.VMEM((tok_rows, width), jnp.float32),
            pltpu.VMEM((tok_rows, LANES), jnp.float32),
            pltpu.VMEM((n_tp, tok_rows, LANES), jnp.float32),
            pltpu.VMEM((depth, cap, width), jnp.bfloat16),
        ]
        + [pltpu.VMEM((slots, count, width), jnp.bfloat16) for slots, count in counts]
        + [pltpu.SemaphoreType.DMA((slots,)) for slots, _ in counts]
        + [
            pltpu.SemaphoreType.DMA((depth,)),
            pltpu.SemaphoreType.DMA((n_tp,)),
            pltpu.SemaphoreType.DMA((n_tp,)),
            pltpu.SemaphoreType.DMA((len(schedule(plans, dims, ())),)),
        ],
        compiler_params=pltpu.CompilerParams(
            collective_id=1, has_side_effects=True, vmem_limit_bytes=VMEM_LIMIT
        ),
        name="scatter_norm",
    )(coef, words, gain, rows)


def body(dims, n_tp, tokens, experts, weights, up_table, out_table, gain):
    n_ep = int(np.prod(dims))
    tok_rows, width = tokens.shape
    cap = 2 * tok_rows * experts.shape[1] // n_ep
    plans = tree_plans(dims, tok_rows)
    rows_held = up_table.shape[0]
    my_words, my_weights = route(experts.T, weights.T, n_ep, cap, rows_held, width // LANES)
    coef, words, rows = collect(
        my_words, my_weights, tokens, up_table, out_table, dims, plans, n_tp, cap
    )
    return scatter_norm(
        coef, words, gain.reshape(1, width), rows, dims, plans, n_tp, tok_rows, lines_of(rows_held, width // LANES)
    )


def solution(mesh):
    placed = (P("ep", "tp"), P("ep", None), P("ep", None), P("ep", "tp"), P("ep", "tp"), P("tp"))
    return jax.shard_map(
        functools.partial(body, ep_dims(mesh), mesh.shape["tp"]),
        mesh=mesh,
        in_specs=placed,
        out_specs=P("ep", "tp"),
        check_vma=False,
    )
```

time: 247 us -> 180 us (0.73)
  Pallas kernels: 231 us -> 177 us
  blocking collectives: 10 us -> 0 us
  other arithmetic: 5.77 us -> 0 us
    pallas_call x5 -> x3, Pallas kernels: 231 us -> 177 us  [the longest x1 86.5 us: collect(): pl.pallas_call(functools.partial(collect_kernel, dims, plans, n_tp), out_...]
    psum x2 -> x0, blocking collectives: 10 us -> none  [the longest x1 5.67 us: body(): dot = lax.psum(partial_dot, 'tp')]
    convert_element_type x2 -> x0, other arithmetic: 3.04 us -> none  [the longest x1 2.18 us: body(): return (mixed * scale[:, None] * gain[None, :]).astype(jnp.bfloat16)]
where the time goes in v2:
time: 180 us; the launch traced here: 179 us
  Pallas kernels  177 us (98%)
  local copies, waits for them, and re-layouts  1.87 us (1%)
    pallas_call x1, Pallas kernels, collect(): pl.pallas_call(functools.partial(collect_kernel, dims, plans, n_tp), out_...  86.5 us
    pallas_call x1, Pallas kernels, scatter_norm(): pl.pallas_call(functools.partial(scatter_kernel, dims, plans, n_tp, lines...  85.8 us
    pallas_call x1, Pallas kernels, route(): pl.pallas_call(functools.partial(route_kernel, n_ep, cap, rows_held, sub)...  5.24 us

profile of v2, /device:TPU:9, one launch (start us, length us, event | category | flops | bytes accessed | tf_op | source)
XLA Modules:
  0.0 179.4 jit_solution(936566621492831968)
XLA Ops:
  0.0 5.2 %route.1 = (s32[16,1,512]{2,1,0:T(1,128)}, f32[16,1,512]{2,1,0:T(1,128)}) custom-call(s32[16,256]{1,0:T(8,128)} %bitcast.3, f32[16,256]{1,0:T(8,128)} %bitcast.4), custom_call_target="tpu_custom_call" | custom-call | tf_op jit(solution)/shard_map/route/pallas_call | solution.py:223
  5.2 86.5 %collect.1 = (f32[16,1,512]{2,1,0:T(1,128)}, s32[16,1,512]{2,1,0:T(1,128)}, bf16[16,512,1024]{2,1,0:T(8,128)(2,1)}) custom-call(s32[16,1,512]{2,1,0:T(1,128)} %get-tuple-element.10.my_word, f32[16,1,512]{2,1,0:T(1,128)} %get-tuple-element.11.my_weight, bf16[256,1024]{1,0:T(8,128)(2,1)} %tok_ref.1, bf16[4096,1024]{1,0:T(8,128)(2,1)} %up_ref.1, ...), custom_call_target="tpu_custom_call" | custom-call | tf_op jit(solution)/shard_map/collect/pallas_call | solution.py:454
  91.7 85.8 %scatter_norm.1 = bf16[256,1024]{1,0:T(8,128)(2,1)} custom-call(f32[16,1,512]{2,1,0:T(1,128)} %get-tuple-element.12.coef_ref, s32[16,1,512]{2,1,0:T(1,128)} %get-tuple-element.13.word_ref, f32[1,1024]{1,0:T(1,128)} %bitcast.5, bf16[16,512,1024]{2,1,0:T(8,128)(2,1)} %get-tuple-element.14.rows_ref), custom_call_target="tpu_custom_call" | custom-call | tf_op jit(solution)/shard_map/scatter_norm/pallas_call | solution.py:693
  177.5 1.9 %copy.8 = bf16[256,1024]{1,0:T(8,128)(2,1)} copy(bf16[256,1024]{1,0:T(8,128)(2,1)} %scatter_norm.1) | data formatting | bytes 1048576

commit v3 on v2

--- a/solution.py
+++ b/solution.py
@@ -14,6 +14,8 @@
 NT = (((1,), (1,)), ((), ()))
 VMEM_LIMIT = 63 * 1024 * 1024
 PITCH = 9
+SPAN = 66.0
+LOAD, TAKE, DOT = 0.35, 0.85, 0.65
 DEPTH = 8
 SCATTER_ORDER = ()
 GATHER_ORDER = (
@@ -185,15 +187,18 @@
     owners = lax.broadcasted_iota(jnp.int32, (n_ep, tok_rows), 0)
     places = lax.broadcasted_iota(jnp.int32, (cap, tok_rows), 0)
     token = lax.broadcasted_iota(jnp.int32, (1, tok_rows), 1)
+    total = jnp.zeros((6 * n_ep, cap), jnp.float32)
+    found = [(experts_ref[k : k + 1, :] // rows_held) == owners for k in range(slots)]
+    ones = jnp.concatenate([jnp.where(mine, 1.0, 0.0) for mine in found], axis=0)
+    ahead_all = jnp.dot(ones.astype(jnp.bfloat16), before, preferred_element_type=jnp.float32)
+    sums = jnp.sum(ones, axis=1, keepdims=True)
     base = jnp.zeros((n_ep, 1), jnp.float32)
-    total = jnp.zeros((6 * n_ep, cap), jnp.float32)
     for k in range(slots):
         e = experts_ref[k : k + 1, :]
         owner = e // rows_held
-        mine = owner == owners
-        ones = jnp.where(mine, 1.0, 0.0)
-        ahead = jnp.dot(ones.astype(jnp.bfloat16), before, preferred_element_type=jnp.float32) + base
-        base = base + jnp.sum(ones, axis=1, keepdims=True)
+        mine = found[k]
+        ahead = ahead_all[k * n_ep : (k + 1) * n_ep, :] + base
+        base = base + sums[k * n_ep : (k + 1) * n_ep, :]
         rank = jnp.sum(jnp.where(mine, ahead, 0.0), axis=0, keepdims=True).astype(jnp.int32)
         at = jnp.where(rank == places, 1.0, 0.0).astype(jnp.bfloat16)
         word = token * rows_held + (e - owner * rows_held)
@@ -249,21 +254,22 @@
     return copy.start, rest
 
 
-def take_rows(row_ref, s, sub, flat, picked, put):
-    cap = row_ref.shape[1]
-    unroll = 32
+def take_rows(row_ref, s, cap, sub, flat, picked, put):
+    batch = 32
     gap = sub + 1 if sub > 1 else 1
-
-    def some(g, carry):
-        taken = []
-        for u in range(unroll):
-            at = row_ref[s, g * unroll + u]
-            taken.append(flat[pl.ds(at, sub, stride=PITCH), :] if sub > 1 else flat[pl.ds(at, 1), :])
-        for u in range(unroll):
-            picked[pl.ds((g * unroll + u) * gap, sub), :] = taken[u]
+    groups = cap // LANES
+
+    def some(q, carry):
+        for g in range(LANES // batch):
+            taken = []
+            for u in range(batch):
+                at = row_ref[s * groups + q, g * batch + u]
+                taken.append(flat[pl.ds(at, sub, stride=PITCH), :] if sub > 1 else flat[pl.ds(at, 1), :])
+            for u in range(batch):
+                picked[pl.ds((q * LANES + g * batch + u) * gap, sub), :] = taken[u]
         return carry
 
-    lax.fori_loop(0, cap // unroll, some, 0)
+    lax.fori_loop(0, groups, some, 0)
     for c in range(sub):
         lines = picked[pl.ds(c, cap, stride=gap), :] if sub > 1 else picked[...]
         put(c, lines.astype(jnp.bfloat16))
@@ -343,7 +349,10 @@
             copy.wait_recv()
         for s in range(n_ep):
             word = word_ref[s]
-            row_held[s : s + 1, :] = word - (word // lines) * lines
+            word = word - (word // lines) * lines
+            for q in range(cap // LANES):
+                at = s * (cap // LANES) + q
+                row_held[at : at + 1, :] = word[:, q * LANES : (q + 1) * LANES]
         copy = pltpu.make_async_copy(row_held, row_ref, row_sem)
         copy.start()
         copy.wait()
@@ -358,14 +367,14 @@
         def put(c, lines):
             packed[s % 2, :, c * LANES : (c + 1) * LANES] = lines
 
-        take_rows(row_ref, s, sub, flat, picked, put)
+        take_rows(row_ref, s, cap, sub, flat, picked, put)
         put_copy(s).start()
 
     def up_rows(s):
         def put(c, lines):
             held[s, :, c * LANES : (c + 1) * LANES] = lines
 
-        take_rows(row_ref, s, sub, flat, picked, put)
+        take_rows(row_ref, s, cap, sub, flat, picked, put)
 
     def dot_of(ranks):
         s = block_of(place, ranks)
@@ -378,12 +387,12 @@
     last = {}
     for i, (v, j, ks) in enumerate(events):
         last[relative(plans, v, ks)] = i
-    work = [(0.3, functools.partial(load, i)) for i in range(pieces)] + [(0.5, lists)]
-    work += [(0.8, functools.partial(out_rows, s)) for s in range(n_ep)]
-    work += [(0.3, functools.partial(load, pieces + i)) for i in range(pieces)]
-    work += [(0.8, functools.partial(up_rows, s)) for s in range(n_ep)]
+    work = [(LOAD, functools.partial(load, i)) for i in range(pieces)] + [(0.5, lists)]
+    work += [(TAKE, functools.partial(out_rows, s)) for s in range(n_ep)]
+    work += [(LOAD, functools.partial(load, pieces + i)) for i in range(pieces)]
+    work += [(TAKE, functools.partial(up_rows, s)) for s in range(n_ep)]
     ready = [(0,) * len(dims)]
-    clock, per_event = 3.0, 62.0 / len(events)
+    clock, per_event = 3.0, SPAN / len(events)
     for i, (v, j, ks) in enumerate(events):
         due = 4.0 + per_event * i
         while clock < due and (work or ready):
@@ -393,7 +402,7 @@
                 clock += cost
             else:
                 dot_of(ready.pop(0))
-                clock += 0.5
+                clock += DOT
         clock = max(clock, due)
         order, first, count = plans[v]
         coords = event_block(place, order, j, ks)
@@ -463,8 +472,8 @@
         scratch_shapes=[
             pltpu.VMEM((n_ep, tok_rows, width), jnp.bfloat16),
             pltpu.VMEM(lists, jnp.float32),
-            pltpu.VMEM((n_ep, cap), jnp.int32),
-            pltpu.SMEM((n_ep, cap), jnp.int32),
+            pltpu.VMEM((n_ep * cap // LANES, LANES), jnp.int32),
+            pltpu.SMEM((n_ep * cap // LANES, LANES), jnp.int32),
             pltpu.VMEM((DEPTH, min(rows_held, 256), width), jnp.bfloat16),
             pltpu.VMEM((lines_of(rows_held, sub), LANES), jnp.float32),
             pltpu.VMEM((cap * (sub + 1 if sub > 1 else 1), LANES), jnp.float32),

time: 180 us -> 159 us (0.88)
  Pallas kernels: 177 us -> 157 us
    pallas_call x1, Pallas kernels: 86.5 us -> 68.2 us  [collect(): pl.pallas_call(functools.partial(collect_kernel, dims, plans, n_tp), out_...]
    pallas_call x1, Pallas kernels: 5.24 us -> 3.03 us  [route(): pl.pallas_call(functools.partial(route_kernel, n_ep, cap, rows_held, sub)...]
where the time goes in v3:
time: 159 us
  Pallas kernels  157 us (99%)
  local copies, waits for them, and re-layouts  1.87 us (1%)
    pallas_call x1, Pallas kernels, scatter_norm(): pl.pallas_call(functools.partial(scatter_kernel, dims, plans, n_tp, lines...  85.9 us
    pallas_call x1, Pallas kernels, collect(): pl.pallas_call(functools.partial(collect_kernel, dims, plans, n_tp), out_...  68.2 us

profile of v3, /device:TPU:9, one launch (start us, length us, event | category | flops | bytes accessed | tf_op | source)
XLA Modules:
  0.0 159.0 jit_solution(16690390649432972559)
XLA Ops:
  0.0 3.0 %route.1 = (s32[16,1,512]{2,1,0:T(1,128)}, f32[16,1,512]{2,1,0:T(1,128)}) custom-call(s32[16,256]{1,0:T(8,128)} %bitcast.3, f32[16,256]{1,0:T(8,128)} %bitcast.4), custom_call_target="tpu_custom_call" | custom-call | tf_op jit(solution)/shard_map/route/pallas_call | solution.py:228
  3.0 68.2 %collect.1 = (f32[16,1,512]{2,1,0:T(1,128)}, s32[16,1,512]{2,1,0:T(1,128)}, bf16[16,512,1024]{2,1,0:T(8,128)(2,1)}) custom-call(s32[16,1,512]{2,1,0:T(1,128)} %get-tuple-element.10.my_word, f32[16,1,512]{2,1,0:T(1,128)} %get-tuple-element.11.my_weight, bf16[256,1024]{1,0:T(8,128)(2,1)} %tok_ref.1, bf16[4096,1024]{1,0:T(8,128)(2,1)} %up_ref.1, ...), custom_call_target="tpu_custom_call" | custom-call | tf_op jit(solution)/shard_map/collect/pallas_call | solution.py:463
  71.2 85.9 %scatter_norm.1 = bf16[256,1024]{1,0:T(8,128)(2,1)} custom-call(f32[16,1,512]{2,1,0:T(1,128)} %get-tuple-element.12.coef_ref, s32[16,1,512]{2,1,0:T(1,128)} %get-tuple-element.13.word_ref, f32[1,1024]{1,0:T(1,128)} %bitcast.5, bf16[16,512,1024]{2,1,0:T(8,128)(2,1)} %get-tuple-element.14.rows_ref), custom_call_target="tpu_custom_call" | custom-call | tf_op jit(solution)/shard_map/scatter_norm/pallas_call | solution.py:702
  157.1 1.9 %copy.8 = bf16[256,1024]{1,0:T(8,128)(2,1)} copy(bf16[256,1024]{1,0:T(8,128)(2,1)} %scatter_norm.1) | data formatting | bytes 1048576
